TPU v7x, 32 devices: a whole 2x2x4 slice. The times are simulated.
32 devices in a mesh: sp: 8 (over z, y), tp: 4 (over x, core).
Axes of the slice: x: 2, y: 2, z: 4, core: 2. Of those that a mesh axis runs over, the one named last changes fastest.
Arguments:
- tokens: bfloat16 [2048, 2048], P('sp'), may hold values from -6 to 6
- input_norm_gain: float32 [2048], replicated, may hold values from 0.1 to 1.9
- convolution_value_weight: bfloat16 [2048, 512], P(None, 'tp'), may hold values from -0.125 to 0.125
- convolution_gate_weight: bfloat16 [2048, 512], P(None, 'tp'), may hold values from -0.125 to 0.125
- depthwise_taps_weight: float32 [31, 512], P(None, 'tp'), may hold values from -1 to 1
- convolution_group_gain: float32 [512], P('tp'), may hold values from 0.1 to 1.9
- convolution_group_shift: float32 [512], P('tp'), may hold values from -3 to 3
- receptance_weight: bfloat16 [2048, 1024], P(None, 'tp'), may hold values from -0.125 to 0.125
- key_weight: bfloat16 [2048, 1024], P(None, 'tp'), may hold values from -0.125 to 0.125
- value_weight: bfloat16 [2048, 1024], P(None, 'tp'), may hold values from -0.125 to 0.125
- decay_weight: bfloat16 [2048, 1024], P(None, 'tp'), may hold values from -0.0625 to 0.0625
- correction_rate_weight: bfloat16 [2048, 1024], P(None, 'tp'), may hold values from -0.125 to 0.125
- output_gate_weight: bfloat16 [2048, 1024], P(None, 'tp'), may hold values from -0.125 to 0.125
- key_prenorm_gain: float32 [1024], P('tp'), may hold values from 0.04 to 8
- decay_offset_bias: float32 [1024], P('tp'), may hold values from -30 to 0
- position_decay_shift: float32 [2048, 1024], P('sp', 'tp'), may hold values from -1 to 1
- extra_log_decay: float32 [2048, 1024], P('sp', 'tp'), may hold values from -0.7 to 0
- head_norm_gain: float32 [1024], P('tp'), may hold values from 0.1 to 1.9
- convolution_output_weight: bfloat16 [512, 2048], replicated, may hold values from -0.15625 to 0.15625
- attention_output_weight: bfloat16 [1024, 2048], replicated, may hold values from -0.15625 to 0.15625
Outputs:
- mixed: bfloat16 [2048, 2048], P(('sp', 'tp'))
All inputs are finite; a program needn't handle non-finite values.
Results may differ from a plain program's by a relative error of at most 0.0063.
The roundings to bfloat16 on the way count: a program that leaves them out, or rounds other values in their place, can miss the bound.
Values may be sent and summed in bfloat16 or wider, within the bound.
A program may use at most 128 MiB of HBM per device.

v0:
```python
import math

import jax
import jax.numpy as jnp
from jax import lax
from jax.sharding import PartitionSpec as P

HEAD = 64


NORM_EPS = 1e-06
GROUP_EPS = 1e-05
HEAD_EPS = 0.00064
KEY_EPS = 1e-06
HIGHEST = lax.Precision.HIGHEST


def from_behind(value, axis, steps):
    count = lax.axis_size(axis)
    leading, last = (max(0, -steps), min(count, count - steps))
    return lax.ppermute(value, axis, [(source, source + steps) for source in range(leading, last)])


def stored(values):
    return lax.optimization_barrier(values.astype(jnp.bfloat16)).astype(jnp.float32)


def einsum_exact(form, left, right):
    return jnp.einsum(form, left, right, precision=HIGHEST)


def to_blocks(values, span_len):
    tok_rows, width = values.shape
    return values.reshape(tok_rows // span_len, span_len, width // HEAD, HEAD).transpose(2, 0, 1, 3)


def block_pass(receptance, decay_logarithm, key_rows, value_rows, unit_key, erase_dir):
    span_len = receptance.shape[2]
    cumulate = jnp.cumsum(decay_logarithm, axis=2)
    before = cumulate - decay_logarithm
    final = cumulate[:, :, -1:, :]
    query_unit = unit_key * jnp.exp(before)
    query_read = receptance * jnp.exp(cumulate)
    scaled_erase = erase_dir * jnp.exp(-cumulate)
    scaled_key = key_rows * jnp.exp(-cumulate)
    strict = jnp.tril(jnp.ones((span_len, span_len), jnp.float32), -1)
    inclusive = jnp.tril(jnp.ones((span_len, span_len), jnp.float32))
    erase_mix = einsum_exact("hbsn,hbjn->hbsj", query_unit, scaled_erase) * strict
    key_mix = einsum_exact("hbsn,hbjn->hbsj", query_unit, scaled_key) * strict
    right_side = jnp.concatenate(
        [-einsum_exact("hbsj,hbjn->hbsn", key_mix, value_rows), -query_unit], axis=-1
    )
    system = erase_mix + jnp.eye(span_len, dtype=jnp.float32)
    removed = jax.scipy.linalg.solve_triangular(system, right_side, lower=True, unit_diagonal=True)
    read_erase = einsum_exact("hbtn,hbjn->hbtj", query_read, scaled_erase) * inclusive
    read_key = einsum_exact("hbtn,hbjn->hbtj", query_read, scaled_key) * inclusive
    readout = einsum_exact("hbtj,hbjr->hbtr", read_erase, removed) + jnp.concatenate(
        [einsum_exact("hbtj,hbjn->hbtn", read_key, value_rows), query_read], axis=-1
    )
    kept_erase = erase_dir * jnp.exp(final - cumulate)
    kept_key = key_rows * jnp.exp(final - cumulate)
    from_removed = einsum_exact("hbjr,hbjn->hbrn", removed, kept_erase)
    local_base = from_removed[:, :, :HEAD] + einsum_exact("hbjv,hbjn->hbvn", value_rows, kept_key)
    transfer = from_removed[:, :, HEAD:] + jnp.eye(HEAD, dtype=jnp.float32) * jnp.exp(final)
    return (readout[..., :HEAD], readout[..., HEAD:], transfer, local_base)


def compose(carry, block):
    trans_now, base_now = carry
    block_trans, block_base = block
    joined = (
        einsum_exact("hij,hjk->hik", trans_now, block_trans),
        einsum_exact("hij,hjk->hik", base_now, block_trans) + block_base,
    )
    return (joined, carry)


def local(
    tokens,
    input_norm_gain,
    convolution_value_weight,
    convolution_gate_weight,
    depthwise_taps_weight,
    convolution_group_gain,
    convolution_group_shift,
    receptance_weight,
    key_weight,
    value_weight,
    decay_weight,
    correction_rate_weight,
    output_gate_weight,
    key_prenorm_gain,
    decay_offset_bias,
    position_decay_shift,
    extra_log_decay,
    head_norm_gain,
    convolution_output_weight,
    attention_output_weight,
):
    tok_rows = tokens.shape[0]
    float_rows = tokens.astype(jnp.float32)
    normed = (
        float_rows
        * lax.rsqrt(jnp.mean(float_rows * float_rows, axis=-1, keepdims=True) + NORM_EPS)
        * input_norm_gain
    ).astype(jnp.bfloat16)

    def project(weight):
        return stored(jnp.dot(normed, weight, preferred_element_type=jnp.float32))

    conv_input = (
        project(convolution_value_weight) * jax.nn.sigmoid(project(convolution_gate_weight))
    ).astype(jnp.bfloat16)
    tap_count = depthwise_taps_weight.shape[0]
    earlier_rows = from_behind(conv_input[tok_rows - tap_count + 1 :], "sp", 1)
    extended = jnp.concatenate([earlier_rows, conv_input], axis=0).astype(jnp.float32)
    conv_sum = jnp.zeros((tok_rows, conv_input.shape[1]), jnp.float32)
    for offset in range(tap_count):
        conv_sum = conv_sum + depthwise_taps_weight[offset] * extended[offset : offset + tok_rows]
    channels = conv_input.shape[1]
    grouped = conv_sum.reshape(tok_rows, channels // 64, 64)
    centred = grouped - jnp.mean(grouped, axis=-1, keepdims=True)
    grouped = centred * lax.rsqrt(jnp.mean(centred * centred, axis=-1, keepdims=True) + GROUP_EPS)
    conv_out = jax.nn.silu(
        grouped.reshape(tok_rows, channels) * convolution_group_gain + convolution_group_shift
    ).astype(jnp.bfloat16)
    span_len = math.gcd(64, tok_rows)
    receptance = project(receptance_weight)
    key_all = project(key_weight)
    value_all = project(value_weight)
    decay_logits = project(decay_weight) + decay_offset_bias + position_decay_shift
    decay_logarithm = -jnp.exp(-jax.nn.softplus(-decay_logits) - 0.5) + extra_log_decay
    erase_rate = jax.nn.sigmoid(project(correction_rate_weight))
    out_gate = jax.nn.sigmoid(project(output_gate_weight))
    unit_key = to_blocks(key_all * key_prenorm_gain, span_len)
    unit_key = unit_key * lax.rsqrt(jnp.sum(unit_key * unit_key, axis=-1, keepdims=True) + KEY_EPS)
    erase_dir = unit_key * to_blocks(erase_rate, span_len)
    local_read, carried_read, transfer, local_base = block_pass(
        to_blocks(receptance, span_len),
        to_blocks(decay_logarithm, span_len),
        to_blocks(key_all, span_len),
        to_blocks(value_all, span_len),
        unit_key,
        erase_dir,
    )
    head_count = transfer.shape[0]
    identity = jnp.broadcast_to(jnp.eye(HEAD, dtype=jnp.float32), (head_count, HEAD, HEAD))
    empty = jnp.zeros((head_count, HEAD, HEAD), jnp.float32)
    totals, priors = lax.scan(
        compose, (identity, empty), (jnp.moveaxis(transfer, 1, 0), jnp.moveaxis(local_base, 1, 0))
    )
    total_trans, total_base = totals
    prior_trans, prior_base = priors
    every_trans, every_base = (
        lax.all_gather(total_trans[None], "sp", axis=0, tiled=True),
        lax.all_gather(total_base[None], "sp", axis=0, tiled=True),
    )
    sp_index = lax.axis_index("sp")

    def absorb(source, state):
        return einsum_exact("hij,hjk->hik", state, every_trans[source]) + every_base[source]

    incoming = lax.fori_loop(0, sp_index, absorb, empty)
    entering = einsum_exact("hij,bhjk->hbik", incoming, prior_trans) + jnp.moveaxis(
        prior_base, 0, 1
    )
    readout = local_read + einsum_exact("hbtk,hbik->hbti", carried_read, entering)
    centred_read = readout - jnp.mean(readout, axis=-1, keepdims=True)
    normed_read = centred_read * lax.rsqrt(
        jnp.mean(centred_read * centred_read, axis=-1, keepdims=True) + HEAD_EPS
    )
    mix_rows = normed_read.transpose(1, 2, 0, 3).reshape(tok_rows, head_count * HEAD)
    mix_out = (mix_rows * head_norm_gain * out_gate).astype(jnp.bfloat16)
    conv_full, mix_full = (
        lax.all_to_all(conv_out, "tp", split_axis=0, concat_axis=1, tiled=True),
        lax.all_to_all(mix_out, "tp", split_axis=0, concat_axis=1, tiled=True),
    )
    projected = jnp.dot(
        conv_full, convolution_output_weight, preferred_element_type=jnp.float32
    ) + jnp.dot(mix_full, attention_output_weight, preferred_element_type=jnp.float32)
    return projected.astype(jnp.bfloat16)


def solution(mesh):
    in_specs = (
        P("sp", None),
        P(),
        P(None, "tp"),
        P(None, "tp"),
        P(None, "tp"),
        P("tp"),
        P("tp"),
        P(None, "tp"),
        P(None, "tp"),
        P(None, "tp"),
        P(None, "tp"),
        P(None, "tp"),
        P(None, "tp"),
        P("tp"),
        P("tp"),
        P("sp", "tp"),
        P("sp", "tp"),
        P("tp"),
        P(),
        P(),
    )
    out_specs = P(("sp", "tp"), None)
    return jax.shard_map(local, mesh=mesh, in_specs=in_specs, out_specs=out_specs, check_vma=False)
```

profile of v0, /device:TPU:28, one launch (start us, length us, event | category | flops | bytes accessed | tf_op | source)
XLA Modules:
  0.0 249.7 jit_solution(3315954925487433820)
XLA Ops:
  1.7 2.0 convolution_convert_fusion.7
  7.9 2.0 convolution_convert_fusion.3
  11.6 2.0 convolution_convert_fusion.2
  14.7 2.0 convolution_convert_fusion.5
  19.3 2.6 %fusion.98 = (f32[4,4,64,64]{3,2,1,0:T(8,128)}, f32[4,4,64,64]{3,2,1,0:T(8,128)S(1)}, f32[4,4,64,64]{3,2,1,0:T(8,128)S(1)}, f32[4,4,64,64]{3,2,1,0:T(8,128)S(1)}) fusion(f32[4,4,64,64]{3,2,1,0:T(8,128)S(1)} %reduce_window_sum.11, f32[4,64,4,64]{3,2,1,0:T(4,128)} %copy-done.5, f32[4,4,64]{2,1,0:T(4,128)S(1)} %add_rsqrt_fusion.1, ...), kind=kLoop, calls=%fused_computation.211 | loop fusion | flops 393216 | bytes 2363392 | tf_op jit(solution)/shard_map/neg | solution.py:51
  21.9 1.8 convolution_multiply_fusion.3
  23.7 1.8 convolution_multiply_fusion
  25.5 1.8 convolution_multiply_fusion.1
  27.4 1.8 fusion.22
  29.2 80.0 %custom-call.4 = f32[4,4,1,64,64]{3,4,2,1,0:T(8,128)} custom-call(f32[4,4,1,64,64]{4,3,2,1,0:T(8,128)} %fusion.22), custom_call_target="InvertDiagBlocksLowerTriangular" | custom-call | tf_op jit(solution)/shard_map/jit(_solve_triangular)/vmap(vmap())/triangular_solve | solution.py:54
  109.2 2.0 convolution_convert_fusion.1
  114.9 2.4 fusion.26
  120.9 2.4 fusion.43
  123.2 2.0 copy.124
  126.4 9.9 %while.28 = (s32[]{:T(128)}, f32[4,64,64]{1,2,0:T(8,128)S(1)}, f32[4,64,64]{1,2,0:T(8,128)S(1)}, f32[4,4,64,64]{2,3,1,0:T(8,128)}, f32[4,4,64,64]{2,3,1,0:T(8,12...) while((s32[]{:T(128)}, f32[4,64,64]{1,2,0:T(8,128)S(1)}, ...), condition=%wide.region_6.7_spmd.clone, body=%wide.region_5.6_spmd.clone.sunk | while | flops 25214980 | bytes 1443436 | solution.py:149
  136.5 34.9 %all-gather = f32[32,64,64]{2,1,0:T(8,128)} all-gather(f32[4,64,64]{2,1,0:T(8,128)S(1)} %copy.94), channel_id=2, replica_groups=mesh['sp'=8,'tp'=4] {'sp'}, dimensions={0}, use_global_device_ids=true | all-gather | bytes 589824 | tf_op jit(solution)/shard_map/all_gather | solution.py:155
  171.4 34.8 %all-gather.1 = f32[32,64,64]{2,1,0:T(8,128)} all-gather(f32[4,64,64]{2,1,0:T(8,128)S(1)} %copy.95), channel_id=3, replica_groups=mesh['sp'=8,'tp'=4] {'sp'}, dimensions={0}, use_global_device_ids=true | all-gather | bytes 589824 | tf_op jit(solution)/shard_map/all_gather | solution.py:156
  206.2 16.9 %while.27 = (s32[]{:T(128)}, f32[4,64,64]{1,2,0:T(8,128)S(1)}, s32[]{:T(128)}, f32[8,4,64,64]{3,2,1,0:T(8,128)}, f32[8,4,64,64]{3,2,1,0:T(8,128)}, /*index=5*/s32[]{:T(128)}, s32[]{:T(128)}, s32[]{:T(128)}) while((s32[]{:T(128)}, f32[4,64,64]{1,2,0:T(8,128)S(1)}, s32[]{:T(128)}, f32[8,4,64,64]{3,2,1,0:T(8,128)}, f32[8,4,64,64]{3,2,1,0:T(8,128)}, ...), condition=%wide.region_8.9_spmd, body=%wide.region_7.8_spmd.sunk | while | flops 12599301 | bytes 721023 | solution.py:163
  223.1 2.0 convolution_add_fusion.2
  230.7 3.3 %all-to-all-start = ((bf16[4,64,128]{2,1,0:T(8,128)(2,1)}), bf16[4,64,128]{2,1,0:T(8,128)(2,1)S(1)}, u32[]{:S(2)}, u32[]{:S(2)}) async-start(bf16[4,64,128]{2,1,0:T(8,128)(2,1)} %bitcast.37), calls=%async_computation | async-start | bytes 131072 | tf_op jit(solution)/shard_map/all_to_all | solution.py:175
  234.7 3.3 %all-to-all-done = bf16[4,64,128]{2,1,0:T(8,128)(2,1)S(1)} async-done(((bf16[4,64,128]{2,1,0:T(8,128)(2,1)}), bf16[4,64,128]{2,1,0:T(8,128)(2,1)S(1)}, u32[]{:S(2)}, u32[]{:S(2)}) %all-to-all-start) | async-done | bytes 65568 | tf_op jit(solution)/shard_map/all_to_all | solution.py:175
  238.0 3.3 %all-to-all-start.1 = ((bf16[4,64,256]{2,1,0:T(8,128)(2,1)}), bf16[4,64,256]{2,1,0:T(8,128)(2,1)S(1)}, u32[]{:S(2)}, u32[]{:S(2)}) async-start(bf16[4,64,256]{2,1,0:T(8,128)(2,1)} %bitcast.61), calls=%async_computation.1 | async-start | bytes 262144 | tf_op jit(solution)/shard_map/all_to_all | solution.py:176
  241.9 4.1 %all-to-all-done.1 = bf16[4,64,256]{2,1,0:T(8,128)(2,1)S(1)} async-done(((bf16[4,64,256]{2,1,0:T(8,128)(2,1)}), bf16[4,64,256]{2,1,0:T(8,128)(2,1)S(1)}, u32[]{:S(2)}, u32[]{:S(2)}) %all-to-all-start.1) | async-done | bytes 131104 | tf_op jit(solution)/shard_map/all_to_all | solution.py:176
  245.9 3.7 %fusion.15 = bf16[64,2048]{1,0:T(8,128)(2,1)} fusion(f32[64,2048]{1,0:T(8,128)S(1)} %fusion.83, bf16[64,1024]{1,0:T(8,128)(2,1)S(1)} %bitcast.224, bf16[1024,2048]{1,0:T(8,128)(2,1)} %param.43), kind=kOutput, calls=%fused_computation.24 | convolution fusion | flops 268697600 | bytes 5111808 | tf_op jit(solution)/shard_map/dot_general | solution.py:180
  (175 shorter events, 52.0 us)
Async XLA Ops:
  0.0 241.4 %copy-start = (bf16[512,2048]{1,0:T(8,128)(2,1)S(1)}, bf16[512,2048]{1,0:T(8,128)(2,1)}, u32[]{:S(2)}) copy-start(bf16[512,2048]{1,0:T(8,128)(2,1)} %param.42) | copy-start | bytes 6291460
  0.0 3.7 %copy-start.9 = (bf16[256,2048]{1,0:T(8,128)(2,1)S(1)}, bf16[256,2048]{1,0:T(8,128)(2,1)}, u32[]{:S(2)}) copy-start(bf16[256,2048]{1,0:T(8,128)(2,1)} %param.24) | copy-start | bytes 3145732
  0.0 3.7 %copy-start.28 = (f32[2048]{0:T(1024)S(1)}, f32[2048]{0:T(1024)}, u32[]{:S(2)}) copy-start(f32[2048]{0:T(1024)} %param.25) | copy-start | bytes 24580
  0.0 3.7 %copy-start.27 = (bf16[2048,128]{1,0:T(8,128)(2,1)S(1)}, bf16[2048,128]{1,0:T(8,128)(2,1)}, u32[]{:S(2)}) copy-start(bf16[2048,128]{1,0:T(8,128)(2,1)} %param.27) | copy-start | bytes 1572868
  1.7 107.5 %copy-start.20 = (f32[256]{0:T(256)}, f32[256]{0:T(256)S(1)}, u32[]{:S(2)}) copy-start(f32[256]{0:T(256)S(1)} %add_rsqrt_fusion.3) | copy-start | bytes 3076
  1.7 4.3 %copy-start.25 = (bf16[2048,256]{1,0:T(8,128)(2,1)S(1)}, bf16[2048,256]{1,0:T(8,128)(2,1)}, u32[]{:S(2)}) copy-start(bf16[2048,256]{1,0:T(8,128)(2,1)} %param.34) | copy-start | bytes 3145732
  4.2 2.3 copy-start.15
  4.2 2.3 copy-start.16
  4.3 224.4 %collective-permute-start = (bf16[30,128]{1,0:T(8,128)(2,1)S(1)}, bf16[30,128]{1,0:T(8,128)(2,1)S(1)}, u32[]{:S(2)}, u32[]{:S(2)}) collective-permute-start(bf16[30,128]{1,0:T(8,128)(2,1)S(1)} %slice.278), channel_id=1, source_target_pairs={{0,4},{4,8},{8,12},{12,16},{16,20},{20,24},{24,28},{1,5},{5,9},{9,... | collective-permute-start | bytes 23048 | tf_op jit(solution)/shard_map/ppermute | solution.py:21
  7.0 3.0 %copy-start.5 = (f32[4,64,4,64]{3,2,1,0:T(4,128)}, f32[4,64,4,64]{3,2,1,0:T(4,128)S(1)}, u32[]{:S(2)}) copy-start(f32[4,64,4,64]{3,2,1,0:T(4,128)S(1)} %reshape.120) | copy-start | bytes 786436
  7.9 3.1 %copy-start.18 = (f32[256]{0:T(256)S(1)}, f32[256]{0:T(256)}, u32[]{:S(2)}) copy-start(f32[256]{0:T(256)} %param.37) | copy-start | bytes 3076
  11.3 3.4 %copy-start.6 = (f32[4,64,4,64]{3,2,1,0:T(4,128)}, f32[4,64,4,64]{3,2,1,0:T(4,128)S(1)}, u32[]{:S(2)}) copy-start(f32[4,64,4,64]{3,2,1,0:T(4,128)S(1)} %reshape.121) | copy-start | bytes 786436
  21.9 5.4 %copy-start.3 = (f32[4,4,64,64]{3,2,1,0:T(8,128)}, f32[4,4,64,64]{3,2,1,0:T(8,128)S(1)}, u32[]{:S(2)}) copy-start(f32[4,4,64,64]{3,2,1,0:T(8,128)S(1)} %get-tuple-element.156) | copy-start | bytes 786436
  113.2 4.1 %copy-start.4 = (f32[4,4,64,64]{3,2,1,0:T(8,128)S(1)}, f32[4,4,64,64]{3,2,1,0:T(8,128)}, u32[]{:S(2)}) copy-start(f32[4,4,64,64]{3,2,1,0:T(8,128)} %copy-done.3) | copy-start | bytes 786436
  114.9 3.5 %copy-start.2 = (f32[4,64,4,64]{3,2,1,0:T(4,128)S(1)}, f32[4,64,4,64]{3,2,1,0:T(4,128)}, u32[]{:S(2)}) copy-start(f32[4,64,4,64]{3,2,1,0:T(4,128)} %reshape.123) | copy-start | bytes 786436
  117.3 2.5 copy-start.7
  206.2 16.9 %copy-start.8 = (f32[4,4,64,128]{3,2,1,0:T(8,128)S(1)}, f32[4,4,64,128]{3,2,1,0:T(8,128)}, u32[]{:S(2)}) copy-start(f32[4,4,64,128]{3,2,1,0:T(8,128)} %copy-done.7) | copy-start | bytes 1572868
  225.1 2.3 copy-start.10
  225.1 2.3 copy-start.21
  225.1 2.3 copy-start.26
  225.2 2.3 copy-start.29
  229.6 4.4 %copy-start.19 = (f32[256]{0:T(256)S(1)}, f32[256]{0:T(256)}, u32[]{:S(2)}) copy-start(f32[256]{0:T(256)} %param.41) | copy-start | bytes 3076
  230.7 7.4 %all-to-all-start = ((bf16[4,64,128]{2,1,0:T(8,128)(2,1)}), bf16[4,64,128]{2,1,0:T(8,128)(2,1)S(1)}, u32[]{:S(2)}, u32[]{:S(2)}) async-start(bf16[4,64,128]{2,1,0:T(8,128)(2,1)} %bitcast.37), calls=%async_computation | async-start | bytes 131072 | tf_op jit(solution)/shard_map/all_to_all | solution.py:175
  238.0 7.9 %all-to-all-start.1 = ((bf16[4,64,256]{2,1,0:T(8,128)(2,1)}), bf16[4,64,256]{2,1,0:T(8,128)(2,1)S(1)}, u32[]{:S(2)}, u32[]{:S(2)}) async-start(bf16[4,64,256]{2,1,0:T(8,128)(2,1)} %bitcast.61), calls=%async_computation.1 | async-start | bytes 262144 | tf_op jit(solution)/shard_map/all_to_all | solution.py:176
  (9 other events, 13.3 us)
where the time goes:
time: 251 us; the launch traced here: 250 us
  other arithmetic  93.6 us (37%)
  blocking collectives  69.6 us (28%)
  matrix products  51.1 us (20%)
  local copies, waits for them, and re-layouts  18.3 us (7%)
  starting transfers between devices  8.03 us (3%)
  waiting for transfers between devices  7.42 us (3%)
    another operation x6, other arithmetic, block_pass(): jax.scipy.linalg.solve_triangular(system, right_side, lower=True, unit_di...  80.1 us
    all_gather x1, blocking collectives, local(): lax.all_gather(total_trans[None], 'sp', axis=0, tiled=True)  34.9 us
    all_gather x1, blocking collectives, local(): lax.all_gather(total_base[None], 'sp', axis=0, tiled=True)  34.8 us
    dot_general x26, matrix products, einsum_exact(): return jnp.einsum(form, left, right, precision=HIGHEST)  32.9 us
    dot_general x8, matrix products, project(): return stored(jnp.dot(normed, weight, preferred_element_type=jnp.float32))  11.6 us
    dynamic_slice x14, local copies, waits for them, and re-layouts, absorb(): every_base[source]  7.14 us
  transfers between devices with their start and end apart: 3, of which 2 were waited for; matrix products, arithmetic and copies ran while one was open for 61% of the time, Pallas kernels for 0%

commit v1 on v0

v1 whole, which is shorter than its diff:
```python
import functools

import jax
import jax.numpy as jnp
from jax import lax
from jax.experimental import pallas as pl
from jax.experimental.pallas import tpu as pltpu
from jax.sharding import PartitionSpec as P

HEAD = 64
CHUNK = 64
PAIR = 128

NORM_EPS = 1e-06
GROUP_EPS = 1e-05
HEAD_EPS = 0.00064
KEY_EPS = 1e-06
MESH = pl.DeviceIdType.MESH
WIRE = jnp.bfloat16
VMEM_LIMIT = 60 * 1024 * 1024
F32 = jnp.float32
BF16 = jnp.bfloat16

NN = (((1,), (0,)), ((), ()))
NT = (((1,), (1,)), ((), ()))
TN = (((0,), (0,)), ((), ()))


def parts(x, count):
    out = []
    for _ in range(count - 1):
        piece = x.astype(BF16)
        out.append(piece)
        x = x - piece.astype(F32)
    out.append(x.astype(BF16))
    return out


def dot(a, b, dims=NN):
    return lax.dot_general(a, b, dims, preferred_element_type=F32)


def mm3(a, b, dims=NN):
    ah, al = parts(a, 2)
    bh, bl = parts(b, 2)
    return dot(ah, bh, dims) + (dot(ah, bl, dims) + dot(al, bh, dims))


def mm_left(a, b, dims=NN, count=2):
    pieces = [dot(piece, b, dims) for piece in parts(a, count)]
    return functools.reduce(jnp.add, pieces)


def mm_right(a, b, dims=NN, count=2):
    pieces = [dot(a, piece, dims) for piece in parts(b, count)]
    return functools.reduce(jnp.add, pieces)


def iota2(rows, cols):
    return (
        lax.broadcasted_iota(jnp.int32, (rows, cols), 0),
        lax.broadcasted_iota(jnp.int32, (rows, cols), 1),
    )


def head_blocks(width):
    row, col = iota2(width, width)
    return (row // HEAD) == (col // HEAD)


def block_diagonal(stacked, width):
    tiled = jnp.concatenate([stacked] * (width // HEAD), axis=0)
    return jnp.where(head_blocks(width), tiled, jnp.zeros_like(tiled))


def local_kernel(
    tok, gain, kgain, bias, shift, extra,
    wcv, wcg, wk, wr, wd, we, wv, wg,
    conv_in, local_out, carried_out, gate_out, tot,
    *scratch,
):
    sources = (wcv, wcg, wk, we, wd, wr, wv, wg)
    buffers, sem = scratch[:8], scratch[8]
    copies = []
    for index, (source, buffer) in enumerate(zip(sources, buffers)):
        copy = pltpu.make_async_copy(source, buffer, sem.at[index])
        copy.start()
        copies.append(copy)
    rows = tok.shape[0]
    width = local_out.shape[1]
    heads = width // HEAD
    pairs = rows // PAIR
    x = tok[...].astype(F32)
    normed = (
        x * lax.rsqrt(jnp.mean(x * x, axis=-1, keepdims=True) + NORM_EPS) * gain[...]
    ).astype(BF16)

    def project(index):
        copies[index].wait()
        return dot(normed, buffers[index][...]).astype(BF16).astype(F32)

    conv_value = project(0)
    conv_in[...] = (conv_value * jax.nn.sigmoid(project(1))).astype(BF16)
    key_all = project(2)
    ones = jnp.where(head_blocks(width), 1.0, 0.0).astype(BF16)
    unit = key_all * kgain[...]
    unit = unit * lax.rsqrt(mm_left(unit * unit, ones) + KEY_EPS)
    erase = unit * jax.nn.sigmoid(project(3))
    logits = project(4) + bias[...] + shift[...]
    decay = jax.nn.sigmoid(logits) * (-0.6065306597126334) + extra[...]
    row, col = iota2(PAIR, PAIR)
    same = (row // CHUNK) == (col // CHUNK)
    strict = same & (row > col)
    inclusive = same & (row >= col)
    eye = jnp.where(row == col, 1.0, 0.0)
    tri = jnp.where(inclusive, 1.0, 0.0).astype(BF16)
    cum = jnp.concatenate(
        [mm_right(tri, decay[p * PAIR:(p + 1) * PAIR], count=3) for p in range(pairs)], axis=0
    )

    def chunk_row(offset):
        return jnp.concatenate(
            [
                jnp.broadcast_to(cum[c + offset:c + offset + 1], (CHUNK, width))
                for c in range(0, rows, CHUNK)
            ],
            axis=0,
        )

    mid = chunk_row(CHUNK // 2 - 1)
    final = chunk_row(CHUNK - 1)
    before = cum - decay
    receptance = project(5)
    value = project(6)
    up = jnp.exp(mid - cum)
    left_unit = unit * jnp.exp(before - mid)
    left_read = receptance * jnp.exp(cum - mid)
    right_erase = erase * up
    right_key = key_all * up
    query_unit = unit * jnp.exp(before)
    query_read = receptance * jnp.exp(cum)
    keep = jnp.exp(final - cum)
    kept_erase = erase * keep
    kept_key = key_all * keep
    gate_out[...] = jax.nn.sigmoid(project(7))

    units = [(h, p) for h in range(heads) for p in range(pairs)]

    def piece(values, unit_index):
        h, p = unit_index
        return values[p * PAIR:(p + 1) * PAIR, h * HEAD:(h + 1) * HEAD]

    lower, read_mix, key_mix, values_of = [], [], [], []
    for u in units:
        left = jnp.concatenate([piece(left_unit, u), piece(left_read, u)], axis=0)
        right = jnp.concatenate([piece(right_erase, u), piece(right_key, u)], axis=0)
        product = mm3(left, right, NT)
        lower.append(jnp.where(strict, product[:PAIR, :PAIR], 0.0))
        key_mix.append(jnp.where(strict, product[:PAIR, PAIR:], 0.0))
        read_mix.append(
            jnp.concatenate(
                [
                    jnp.where(inclusive, product[PAIR:, :PAIR], 0.0),
                    jnp.where(inclusive, product[PAIR:, PAIR:], 0.0),
                ],
                axis=1,
            )
        )
        values_of.append(piece(value, u))
    right_side = [
        -jnp.concatenate([mm_left(k, v.astype(BF16)), piece(query_unit, u)], axis=1)
        for k, v, u in zip(key_mix, values_of, units)
    ]
    first = strict & ((row // 2) == (col // 2))
    inverse = [eye - jnp.where(first, low, 0.0) for low in lower]
    size = 2
    while size < CHUNK:
        level = ((row // (2 * size)) == (col // (2 * size))) & ((row // size) > (col // size))
        inner = [mm3(jnp.where(level, low, 0.0), inv) for low, inv in zip(lower, inverse)]
        inverse = [inv - mm3(inv, step) for inv, step in zip(inverse, inner)]
        size *= 2
    removed = [mm3(inv, rhs) for inv, rhs in zip(inverse, right_side)]
    zeros = jnp.zeros((PAIR, HEAD), F32)
    readout = []
    for mix, rem, val, u in zip(read_mix, removed, values_of, units):
        stacked = jnp.concatenate([rem, jnp.concatenate([val, zeros], axis=1)], axis=0)
        readout.append(
            mm3(mix, stacked) + jnp.concatenate([zeros, piece(query_read, u)], axis=1)
        )
    eye_head = iota2(HEAD, HEAD)
    eye_head = eye_head[0] == eye_head[1]
    for h in range(heads):
        state = None
        for p in range(pairs):
            index = h * pairs + p
            ke, kk = piece(kept_erase, (h, p)), piece(kept_key, (h, p))
            for half in range(PAIR // CHUNK):
                span = slice(half * CHUNK, (half + 1) * CHUNK)
                start = p * PAIR + half * CHUNK
                lanes = slice(h * HEAD, (h + 1) * HEAD)
                read = readout[index][span]
                if state is not None:
                    read = jnp.concatenate(
                        [read[:, :HEAD], jnp.zeros((CHUNK, HEAD), F32)], axis=1
                    ) + mm3(read[:, HEAD:], state, NT)
                local_out[start:start + CHUNK, lanes] = read[:, :HEAD]
                carried_out[start:start + CHUNK, lanes] = read[:, HEAD:]
                from_removed = mm3(removed[index][span], ke[span], TN)
                base = from_removed[:HEAD] + mm3(values_of[index][span], kk[span], TN)
                last = jnp.exp(final[start:start + 1, lanes])
                trans = from_removed[HEAD:] + jnp.where(eye_head, last, 0.0)
                if state is None:
                    state = jnp.concatenate([base, trans], axis=0)
                else:
                    moved = mm3(state, trans)
                    state = jnp.concatenate([moved[:HEAD] + base, moved[HEAD:]], axis=0)
        tot[:, h * HEAD:(h + 1) * HEAD] = state.astype(tot.dtype)


def exchange_kernel(
    n_sp, n_tp,
    conv_in, taps, ggain, gshift, local_read, carried, gate, tot, hgain, wco, wao,
    out,
    wco_buf, wao_buf, extended, halo, partner_map, pair_map, maps, state,
    conv_out, mix_out, conv_slots, mix_slots,
    weight_sem, halo_sem, pair_sem, map_send, map_recv, conv_send, conv_recv, mix_send, mix_recv,
):
    sp, tp = lax.axis_index("sp"), lax.axis_index("tp")
    weight_copies = [
        pltpu.make_async_copy(wco, wco_buf, weight_sem.at[0]),
        pltpu.make_async_copy(wao, wao_buf, weight_sem.at[1]),
    ]
    for copy in weight_copies:
        copy.start()
    barrier = pltpu.get_barrier_semaphore()
    for step in range(1, n_sp):
        pl.semaphore_signal(
            barrier, inc=1, device_id=(lax.rem(sp + step, n_sp), tp), device_id_type=MESH
        )
    for step in range(1, n_tp):
        pl.semaphore_signal(
            barrier, inc=1, device_id=(sp, lax.rem(tp + step, n_tp)), device_id_type=MESH
        )
    pl.semaphore_wait(barrier, n_sp + n_tp - 2)

    rows, channels = conv_in.shape
    width = local_read.shape[1]
    halo_rows = halo.shape[0]
    groups = n_sp // 2
    group, parity = sp // 2, lax.rem(sp, 2)
    first_member = parity == 0

    pair_copy = pltpu.make_async_remote_copy(
        src_ref=tot, dst_ref=partner_map, send_sem=pair_sem.at[0], recv_sem=pair_sem.at[1],
        device_id=(sp + 1 - 2 * parity, tp), device_id_type=MESH,
    )
    pair_copy.start()
    halo_copy = pltpu.make_async_remote_copy(
        src_ref=conv_in.at[pl.ds(rows - halo_rows, halo_rows)], dst_ref=halo,
        send_sem=halo_sem.at[0], recv_sem=halo_sem.at[1],
        device_id=(lax.rem(sp + 1, n_sp), tp), device_id_type=MESH,
    )
    halo_copy.start()
    extended[halo_rows:, :] = conv_in[...].astype(F32)

    def chain(carry, block):
        trans = block_diagonal(block[HEAD:].astype(F32), width).astype(BF16)
        return mm_left(carry, trans) if WIRE == BF16 else mm3(
            carry, block_diagonal(block[HEAD:].astype(F32), width))

    pair_copy.wait()
    mine, theirs = tot[...].astype(F32), partner_map[...].astype(F32)
    early = jnp.where(first_member, mine, theirs)
    late = jnp.where(first_member, theirs, mine)
    joined = chain(early, late)
    pair_map[:HEAD] = (joined[:HEAD] + late[:HEAD]).astype(pair_map.dtype)
    pair_map[HEAD:] = joined[HEAD:].astype(pair_map.dtype)

    def map_copy(ahead):
        return pltpu.make_async_remote_copy(
            src_ref=pair_map, dst_ref=maps.at[ahead],
            send_sem=map_send.at[ahead], recv_sem=map_recv.at[ahead],
            device_id=(sp + 2 * ahead, tp), device_id_type=MESH,
        )

    for ahead in range(1, groups):
        @pl.when(group + ahead < groups)
        def _():
            map_copy(ahead).start()

    halo_copy.wait()
    received = halo[...].astype(F32)
    extended[:halo_rows, :] = jnp.where(sp == 0, 0.0, received)
    tap_count = taps.shape[0]
    total = jnp.zeros((rows, channels), F32)
    for offset in range(tap_count):
        begin = halo_rows - tap_count + 1 + offset
        total = total + taps[offset:offset + 1, :] * extended[begin:begin + rows, :]
    means = jnp.where(head_blocks(channels), 1.0 / HEAD, 0.0).astype(BF16)
    centred = total - mm_left(total, means)
    scaled = centred * lax.rsqrt(mm_left(centred * centred, means) + GROUP_EPS)
    conv_out[...] = jax.nn.silu(scaled * ggain[...] + gshift[...]).astype(BF16)

    span = rows // n_tp

    def spread(source, slots, send, recv):
        copies = []
        for step in range(1, n_tp):
            target = lax.rem(tp + step, n_tp)
            begin = pl.multiple_of(target * span, span)
            copy = pltpu.make_async_remote_copy(
                src_ref=source.at[pl.ds(begin, span)], dst_ref=slots.at[step],
                send_sem=send.at[step], recv_sem=recv.at[step],
                device_id=(sp, target), device_id_type=MESH,
            )
            copy.start()
            copies.append(copy)
        return copies

    conv_copies = spread(conv_out, conv_slots, conv_send, conv_recv)

    state[...] = jnp.zeros_like(state)
    for ahead in range(groups - 1, 0, -1):
        @pl.when(group >= ahead)
        def _():
            map_copy(ahead).wait_recv()
            block = maps[ahead]
            state[...] = chain(state[...], block) + block[:HEAD].astype(F32)

    behind = chain(state[...], early) + early[:HEAD]
    entering = jnp.where(first_member, state[...], behind)
    readout = local_read[...] + mm3(carried[...], block_diagonal(entering, width), NT)
    head_means = jnp.where(head_blocks(width), 1.0 / HEAD, 0.0).astype(BF16)
    centred = readout - mm_left(readout, head_means)
    scaled = centred * lax.rsqrt(mm_left(centred * centred, head_means) + HEAD_EPS)
    mix_out[...] = (scaled * hgain[...] * gate[...]).astype(BF16)
    mix_copies = spread(mix_out, mix_slots, mix_send, mix_recv)

    own = pl.multiple_of(tp * span, span)
    for copy in weight_copies:
        copy.wait()

    def gather(result, source, slots, copies, weight, depth):
        result = result + dot(
            source[pl.ds(own, span)], weight[pl.ds(pl.multiple_of(tp * depth, depth), depth)]
        )
        for step in range(1, n_tp):
            copies[step - 1].wait_recv()
            begin = lax.rem(tp - step + n_tp, n_tp) * depth
            result = result + dot(
                slots[step], weight[pl.ds(pl.multiple_of(begin, depth), depth)]
            )
        return result

    result = gather(
        jnp.zeros(out.shape, F32), conv_out, conv_slots, conv_copies, wco_buf, channels
    )
    result = gather(result, mix_out, mix_slots, mix_copies, wao_buf, width)
    out[...] = result.astype(BF16)
    for copy in conv_copies + mix_copies:
        copy.wait_send()
    for ahead in range(1, groups):
        @pl.when(group + ahead < groups)
        def _():
            map_copy(ahead).wait_send()


def local(
    n_sp, n_tp,
    tokens, input_norm_gain, convolution_value_weight, convolution_gate_weight,
    depthwise_taps_weight, convolution_group_gain, convolution_group_shift,
    receptance_weight, key_weight, value_weight, decay_weight, correction_rate_weight,
    output_gate_weight, key_prenorm_gain, decay_offset_bias, position_decay_shift,
    extra_log_decay, head_norm_gain, convolution_output_weight, attention_output_weight,
):
    rows, model = tokens.shape
    channels = convolution_value_weight.shape[1]
    width = key_weight.shape[1]
    vmem = pl.BlockSpec(memory_space=pltpu.VMEM)
    anywhere = pl.BlockSpec(memory_space=pl.ANY)

    def line(values):
        return values.reshape(1, -1)

    weight_shapes = [(model, channels)] * 2 + [(model, width)] * 6
    conv_in, local_read, carried, gate, tot = pl.pallas_call(
        local_kernel,
        name="local_pass",
        out_shape=(
            jax.ShapeDtypeStruct((rows, channels), BF16),
            jax.ShapeDtypeStruct((rows, width), F32),
            jax.ShapeDtypeStruct((rows, width), F32),
            jax.ShapeDtypeStruct((rows, width), F32),
            jax.ShapeDtypeStruct((2 * HEAD, width), WIRE),
        ),
        in_specs=[vmem] * 6 + [anywhere] * 8,
        out_specs=(vmem,) * 5,
        scratch_shapes=[pltpu.VMEM(shape, BF16) for shape in weight_shapes]
        + [pltpu.SemaphoreType.DMA((8,))],
        compiler_params=pltpu.CompilerParams(vmem_limit_bytes=VMEM_LIMIT),
    )(
        tokens, line(input_norm_gain), line(key_prenorm_gain), line(decay_offset_bias),
        position_decay_shift, extra_log_decay,
        convolution_value_weight, convolution_gate_weight, key_weight, receptance_weight,
        decay_weight, correction_rate_weight, value_weight, output_gate_weight,
    )
    span = rows // n_tp
    halo_rows = -(-(depthwise_taps_weight.shape[0] - 1) // 16) * 16
    groups = n_sp // 2
    dma = pltpu.SemaphoreType.DMA
    return pl.pallas_call(
        functools.partial(exchange_kernel, n_sp, n_tp),
        name="exchange_pass",
        out_shape=jax.ShapeDtypeStruct((span, model), BF16),
        in_specs=[vmem] * 9 + [anywhere] * 2,
        out_specs=vmem,
        scratch_shapes=[
            pltpu.VMEM(convolution_output_weight.shape, BF16),
            pltpu.VMEM(attention_output_weight.shape, BF16),
            pltpu.VMEM((halo_rows + rows, channels), F32),
            pltpu.VMEM((halo_rows, channels), BF16),
            pltpu.VMEM((2 * HEAD, width), WIRE),
            pltpu.VMEM((2 * HEAD, width), WIRE),
            pltpu.VMEM((groups, 2 * HEAD, width), WIRE),
            pltpu.VMEM((HEAD, width), F32),
            pltpu.VMEM((rows, channels), BF16),
            pltpu.VMEM((rows, width), BF16),
            pltpu.VMEM((n_tp, span, channels), BF16),
            pltpu.VMEM((n_tp, span, width), BF16),
            dma((2,)), dma((2,)), dma((2,)), dma((groups,)), dma((groups,)),
            dma((n_tp,)), dma((n_tp,)), dma((n_tp,)), dma((n_tp,)),
        ],
        compiler_params=pltpu.CompilerParams(
            collective_id=0, has_side_effects=True, vmem_limit_bytes=VMEM_LIMIT
        ),
    )(
        conv_in, depthwise_taps_weight, line(convolution_group_gain),
        line(convolution_group_shift), local_read, carried, gate, tot, line(head_norm_gain),
        convolution_output_weight, attention_output_weight,
    )


def solution(mesh):
    in_specs = (
        P("sp", None),
        P(),
        P(None, "tp"),
        P(None, "tp"),
        P(None, "tp"),
        P("tp"),
        P("tp"),
        P(None, "tp"),
        P(None, "tp"),
        P(None, "tp"),
        P(None, "tp"),
        P(None, "tp"),
        P(None, "tp"),
        P("tp"),
        P("tp"),
        P("sp", "tp"),
        P("sp", "tp"),
        P("tp"),
        P(),
        P(),
    )
    body = functools.partial(local, mesh.shape["sp"], mesh.shape["tp"])
    return jax.shard_map(
        body, mesh=mesh, in_specs=in_specs, out_specs=P(("sp", "tp"), None), check_vma=False
    )
```

time: 251 us -> 38.2 us (0.15)
  the two profiles are of different devices: /device:TPU:28 before, /device:TPU:25 now
where the time goes in v1:
time: 38.2 us; the launch traced here: 38 us
  Pallas kernels  36.3 us (95%)
  local copies, waits for them, and re-layouts  1.67 us (4%)
    pallas_call x1, Pallas kernels, local(): pl.pallas_call(functools.partial(exchange_kernel, n_sp, n_tp), name='exch...  20.3 us
    pallas_call x1, Pallas kernels, local(): pl.pallas_call(local_kernel, name='local_pass', out_shape=(jax.ShapeDtype...  16 us
    unnamed x1, local copies, waits for them, and re-layouts  1.67 us

profile of v1, /device:TPU:25, one launch (start us, length us, event | category | flops | bytes accessed | tf_op | source)
XLA Modules:
  0.0 38.0 jit_solution(17271515625157139681)
XLA Ops:
  0.0 16.0 %local_pass.1 = (bf16[256,128]{1,0:T(8,128)(2,1)}, f32[256,256]{1,0:T(8,128)}, f32[256,256]{1,0:T(8,128)}, f32[256,256]{1,0:T(8,128)}, bf16[128,256]{1,0:T(8,128)(2,1)}) custom-call(bf16[256,2048]{1,0:T(8,128)(2,1)} %tok.1, f32[1,2048]{1,0:T(1,128)} %bitcast.6, f32[1,256]{1,0:T(1,128)} %bitcast.7, f32[1,256]{1,0:T(1,128)} %bitcast.8, f32[256,256]{1,0:T(8,128)} %shift.1, ...), custom_call_target="tpu_custom_call" | custom-call | tf_op jit(solution)/shard_map/local_pass/pallas_call | solution.py:386
  16.0 20.3 %exchange_pass.1 = bf16[64,2048]{1,0:T(8,128)(2,1)} custom-call(bf16[256,128]{1,0:T(8,128)(2,1)} %get-tuple-element.10.conv_in, f32[31,128]{1,0:T(8,128)} %taps.1, f32[1,128]{1,0:T(1,128)} %bitcast.10, f32[1,128]{1,0:T(1,128)} %bitcast.11, f32[256,256]{1,0:T(8,128)} %get-tuple-element.11.local_read, f32[256,256]{1,0:T(8,128)} %get-tuple-element.12.carried, ...), custom_call_target="tpu_custom_call" | custom-call | tf_op jit(solution)/shard_map/exchange_pass/pallas_call | solution.py:411
  36.3 1.7 %copy.22 = bf16[64,2048]{1,0:T(8,128)(2,1)} copy(bf16[64,2048]{1,0:T(8,128)(2,1)} %exchange_pass.1) | data formatting | bytes 524288

commit v2 on v1

v2 whole, which is shorter than its diff:
```python
import functools

import jax
import jax.numpy as jnp
from jax import lax
from jax.experimental import pallas as pl
from jax.experimental.pallas import tpu as pltpu
from jax.sharding import PartitionSpec as P

HEAD = 64
CHUNK = 64
PAIR = 128

NORM_EPS = 1e-06
GROUP_EPS = 1e-05
HEAD_EPS = 0.00064
KEY_EPS = 1e-06
MESH = pl.DeviceIdType.MESH
WIRE = jnp.bfloat16
VMEM_LIMIT = 60 * 1024 * 1024
F32 = jnp.float32
BF16 = jnp.bfloat16

NN = (((1,), (0,)), ((), ()))
NT = (((1,), (1,)), ((), ()))
TN = (((0,), (0,)), ((), ()))


def parts(x, count):
    out = []
    for _ in range(count - 1):
        piece = x.astype(BF16)
        out.append(piece)
        x = x - piece.astype(F32)
    out.append(x.astype(BF16))
    return out


def dot(a, b, dims=NN):
    return lax.dot_general(a, b, dims, preferred_element_type=F32)


def mm3(a, b, dims=NN):
    ah, al = parts(a, 2)
    bh, bl = parts(b, 2)
    return dot(ah, bh, dims) + (dot(ah, bl, dims) + dot(al, bh, dims))


def mm_left(a, b, dims=NN, count=2):
    pieces = [dot(piece, b, dims) for piece in parts(a, count)]
    return functools.reduce(jnp.add, pieces)


def mm_right(a, b, dims=NN, count=2):
    pieces = [dot(a, piece, dims) for piece in parts(b, count)]
    return functools.reduce(jnp.add, pieces)


PASSES = dict(qk=3, kmv=2, inv=1, rem=1, res=3, fix=1, read=3, keep=3, state=3, carry=3, enter=3)
REFINE = True


def mm(a, b, site, dims=NN):
    passes = PASSES[site]
    if passes == 1:
        return dot(a.astype(BF16), b.astype(BF16), dims)
    if passes == 2:
        return mm_left(a, b.astype(BF16), dims)
    return mm3(a, b, dims)


def iota2(rows, cols):
    return (
        lax.broadcasted_iota(jnp.int32, (rows, cols), 0),
        lax.broadcasted_iota(jnp.int32, (rows, cols), 1),
    )


def head_blocks(width):
    row, col = iota2(width, width)
    return (row // HEAD) == (col // HEAD)


def block_diagonal(stacked, width):
    tiled = jnp.concatenate([stacked] * (width // HEAD), axis=0)
    return jnp.where(head_blocks(width), tiled, jnp.zeros_like(tiled))


def layer_kernel(
    n_sp, n_tp,
    tok, gain, kgain, bias, shift, extra, taps, ggain, gshift, hgain,
    wcv, wcg, wk, wr, wd, we, wv, wg, wco, wao,
    out,
    cv_buf, cg_buf, k_buf, r_buf, d_buf, e_buf, v_buf, g_buf, co_buf, ao_buf,
    conv_in, extended, halo, own_map, partner_map, pair_map, maps, state,
    local_read, carried, conv_out, mix_out, conv_slots, mix_slots,
    weight_sem, halo_sem, pair_sem, map_send, map_recv, conv_send, conv_recv, mix_send, mix_recv,
):
    sp, tp = lax.axis_index("sp"), lax.axis_index("tp")
    barrier = pltpu.get_barrier_semaphore()
    for step in range(1, n_sp):
        pl.semaphore_signal(
            barrier, inc=1, device_id=(lax.rem(sp + step, n_sp), tp), device_id_type=MESH
        )
    for step in range(1, n_tp):
        pl.semaphore_signal(
            barrier, inc=1, device_id=(sp, lax.rem(tp + step, n_tp)), device_id_type=MESH
        )
    order = (
        (wk, k_buf), (we, e_buf), (wd, d_buf), (wv, v_buf), (wcv, cv_buf), (wcg, cg_buf),
        (wr, r_buf), (wg, g_buf), (wco, co_buf), (wao, ao_buf),
    )
    copies = []
    for index, (source, buffer) in enumerate(order):
        copy = pltpu.make_async_copy(source, buffer, weight_sem.at[index])
        copy.start()
        copies.append(copy)
    rows = tok.shape[0]
    channels = conv_in.shape[1]
    width = local_read.shape[1]
    heads = width // HEAD
    pairs = rows // PAIR
    halo_rows = halo.shape[0]
    groups = n_sp // 2
    group, parity = sp // 2, lax.rem(sp, 2)
    first_member = parity == 0
    x = tok[...].astype(F32)
    normed = (
        x * lax.rsqrt(jnp.mean(x * x, axis=-1, keepdims=True) + NORM_EPS) * gain[...]
    ).astype(BF16)

    def project(index):
        copies[index].wait()
        return dot(normed, order[index][1][...]).astype(BF16).astype(F32)

    key_all = project(0)
    ones = jnp.where(head_blocks(width), 1.0, 0.0).astype(BF16)
    unit = key_all * kgain[...]
    unit = unit * lax.rsqrt(mm_left(unit * unit, ones) + KEY_EPS)
    erase = unit * jax.nn.sigmoid(project(1))
    logits = project(2) + bias[...] + shift[...]
    decay = jax.nn.sigmoid(logits) * (-0.6065306597126334) + extra[...]
    row, col = iota2(PAIR, PAIR)
    same = (row // CHUNK) == (col // CHUNK)
    strict = same & (row > col)
    inclusive = same & (row >= col)
    eye = jnp.where(row == col, 1.0, 0.0)
    tri = jnp.where(inclusive, 1.0, 0.0).astype(BF16)
    cum = jnp.concatenate(
        [mm_right(tri, decay[p * PAIR:(p + 1) * PAIR], count=3) for p in range(pairs)], axis=0
    )

    def chunk_row(offset):
        return jnp.concatenate(
            [
                jnp.broadcast_to(cum[c + offset:c + offset + 1], (CHUNK, width))
                for c in range(0, rows, CHUNK)
            ],
            axis=0,
        )

    mid = chunk_row(CHUNK // 2 - 1)
    final = chunk_row(CHUNK - 1)
    before = cum - decay
    up = jnp.exp(mid - cum)
    left_unit = unit * jnp.exp(before - mid)
    right_erase = erase * up
    right_key = key_all * up
    query_unit = unit * jnp.exp(before)
    keep = jnp.exp(final - cum)
    kept_erase = erase * keep
    kept_key = key_all * keep
    value = project(3)

    units = [(h, p) for h in range(heads) for p in range(pairs)]

    def piece(values, unit_index):
        h, p = unit_index
        return values[p * PAIR:(p + 1) * PAIR, h * HEAD:(h + 1) * HEAD]

    lower, key_mix, values_of, rights = [], [], [], []
    for u in units:
        right = jnp.concatenate([piece(right_erase, u), piece(right_key, u)], axis=0)
        product = mm(piece(left_unit, u), right, "qk", NT)
        lower.append(jnp.where(strict, product[:, :PAIR], 0.0))
        key_mix.append(jnp.where(strict, product[:, PAIR:], 0.0))
        values_of.append(piece(value, u))
        rights.append(right)
    right_side = [
        -jnp.concatenate([mm(k, v, "kmv"), piece(query_unit, u)], axis=1)
        for k, v, u in zip(key_mix, values_of, units)
    ]
    first = strict & ((row // 2) == (col // 2))
    inverse = [eye - jnp.where(first, low, 0.0) for low in lower]
    size = 2
    while size < CHUNK:
        level = ((row // (2 * size)) == (col // (2 * size))) & ((row // size) > (col // size))
        inner = [mm(jnp.where(level, low, 0.0), inv, "inv") for low, inv in zip(lower, inverse)]
        inverse = [inv - mm(inv, step, "inv") for inv, step in zip(inverse, inner)]
        size *= 2
    removed = [mm(inv, rhs, "rem") for inv, rhs in zip(inverse, right_side)]
    if REFINE:
        left_over = [
            rhs - rem - mm(low, rem, "res") for rhs, rem, low in zip(right_side, removed, lower)
        ]
        removed = [
            rem + mm(inv, rest, "fix") for rem, inv, rest in zip(removed, inverse, left_over)
        ]
    eye_head = iota2(HEAD, HEAD)
    eye_head = eye_head[0] == eye_head[1]
    blocks = {}
    for h in range(heads):
        for p in range(pairs):
            index = h * pairs + p
            ke, kk = piece(kept_erase, (h, p)), piece(kept_key, (h, p))
            for half in range(PAIR // CHUNK):
                span = slice(half * CHUNK, (half + 1) * CHUNK)
                start = p * PAIR + half * CHUNK
                from_removed = mm(removed[index][span], ke[span], "keep", TN)
                base = from_removed[:HEAD] + mm(values_of[index][span], kk[span], "keep", TN)
                last = jnp.exp(final[start:start + 1, h * HEAD:(h + 1) * HEAD])
                trans = from_removed[HEAD:] + jnp.where(eye_head, last, 0.0)
                blocks[h, start // CHUNK] = (base, trans)
    priors = {}
    totals = [None] * heads
    for chunk in range(rows // CHUNK):
        for h in range(heads):
            base, trans = blocks[h, chunk]
            priors[h, chunk] = totals[h]
            if totals[h] is None:
                totals[h] = jnp.concatenate([base, trans], axis=0)
            else:
                moved = mm(totals[h], trans, "state")
                totals[h] = jnp.concatenate([moved[:HEAD] + base, moved[HEAD:]], axis=0)
    own_total = jnp.concatenate(totals, axis=1).astype(WIRE)
    own_map[...] = own_total

    pl.semaphore_wait(barrier, n_sp + n_tp - 2)
    pair_copy = pltpu.make_async_remote_copy(
        src_ref=own_map, dst_ref=partner_map, send_sem=pair_sem.at[0], recv_sem=pair_sem.at[1],
        device_id=(sp + 1 - 2 * parity, tp), device_id_type=MESH,
    )
    pair_copy.start()

    conv_value = project(4)
    conv_rows = (conv_value * jax.nn.sigmoid(project(5))).astype(BF16)
    conv_in[...] = conv_rows
    halo_copy = pltpu.make_async_remote_copy(
        src_ref=conv_in.at[pl.ds(rows - halo_rows, halo_rows)], dst_ref=halo,
        send_sem=halo_sem.at[0], recv_sem=halo_sem.at[1],
        device_id=(lax.rem(sp + 1, n_sp), tp), device_id_type=MESH,
    )
    halo_copy.start()
    extended[halo_rows:, :] = conv_rows.astype(F32)

    def chain(carry, block):
        trans = block_diagonal(block[HEAD:], width)
        return mm(carry, trans, "enter")

    receptance = project(6)
    left_read = receptance * jnp.exp(cum - mid)
    query_read = receptance * jnp.exp(cum)

    pair_copy.wait()
    mine, theirs = own_total.astype(F32), partner_map[...].astype(F32)
    early = jnp.where(first_member, mine, theirs)
    late = jnp.where(first_member, theirs, mine)
    joined = chain(early, late)
    pair_map[:HEAD] = (joined[:HEAD] + late[:HEAD]).astype(WIRE)
    pair_map[HEAD:] = joined[HEAD:].astype(WIRE)

    def map_copy(ahead):
        return pltpu.make_async_remote_copy(
            src_ref=pair_map, dst_ref=maps.at[ahead],
            send_sem=map_send.at[ahead], recv_sem=map_recv.at[ahead],
            device_id=(sp + 2 * ahead, tp), device_id_type=MESH,
        )

    for ahead in range(1, groups):
        @pl.when(group + ahead < groups)
        def _():
            map_copy(ahead).start()

    halo_copy.wait()
    received = halo[...].astype(F32)
    extended[:halo_rows, :] = jnp.where(sp == 0, 0.0, received)
    tap_count = taps.shape[0]
    total = jnp.zeros((rows, channels), F32)
    for offset in range(tap_count):
        begin = halo_rows - tap_count + 1 + offset
        total = total + taps[offset:offset + 1, :] * extended[begin:begin + rows, :]
    means = jnp.where(head_blocks(channels), 1.0 / HEAD, 0.0).astype(BF16)
    centred = total - mm_left(total, means)
    scaled = centred * lax.rsqrt(mm_left(centred * centred, means) + GROUP_EPS)
    conv_out[...] = jax.nn.silu(scaled * ggain[...] + gshift[...]).astype(BF16)

    span = rows // n_tp

    def spread(source, slots, send, recv):
        started = []
        for step in range(1, n_tp):
            target = lax.rem(tp + step, n_tp)
            begin = pl.multiple_of(target * span, span)
            copy = pltpu.make_async_remote_copy(
                src_ref=source.at[pl.ds(begin, span)], dst_ref=slots.at[step],
                send_sem=send.at[step], recv_sem=recv.at[step],
                device_id=(sp, target), device_id_type=MESH,
            )
            copy.start()
            started.append(copy)
        return started

    conv_copies = spread(conv_out, conv_slots, conv_send, conv_recv)

    zeros = jnp.zeros((PAIR, HEAD), F32)
    for index, u in enumerate(units):
        h, p = u
        product = mm(piece(left_read, u), rights[index], "qk", NT)
        mix = jnp.concatenate(
            [
                jnp.where(inclusive, product[:, :PAIR], 0.0),
                jnp.where(inclusive, product[:, PAIR:], 0.0),
            ],
            axis=1,
        )
        stacked = jnp.concatenate(
            [removed[index], jnp.concatenate([values_of[index], zeros], axis=1)], axis=0
        )
        readout = mm(mix, stacked, "read") + jnp.concatenate(
            [zeros, piece(query_read, u)], axis=1
        )
        for half in range(PAIR // CHUNK):
            start = p * PAIR + half * CHUNK
            lanes = slice(h * HEAD, (h + 1) * HEAD)
            read = readout[half * CHUNK:(half + 1) * CHUNK]
            prior = priors[h, start // CHUNK]
            if prior is not None:
                read = jnp.concatenate(
                    [read[:, :HEAD], jnp.zeros((CHUNK, HEAD), F32)], axis=1
                ) + mm(read[:, HEAD:], prior, "carry", NT)
            local_read[start:start + CHUNK, lanes] = read[:, :HEAD]
            carried[start:start + CHUNK, lanes] = read[:, HEAD:]
    gate = jax.nn.sigmoid(project(7)) * hgain[...]

    own = pl.multiple_of(tp * span, span)

    def gather(result, source, slots, arriving, weight, depth):
        result = result + dot(
            source[pl.ds(own, span)], weight[pl.ds(pl.multiple_of(tp * depth, depth), depth)]
        )
        for step in range(1, n_tp):
            arriving[step - 1].wait_recv()
            begin = lax.rem(tp - step + n_tp, n_tp) * depth
            result = result + dot(
                slots[step], weight[pl.ds(pl.multiple_of(begin, depth), depth)]
            )
        return result

    copies[8].wait()
    result = gather(
        jnp.zeros(out.shape, F32), conv_out, conv_slots, conv_copies, co_buf, channels
    )

    state[...] = jnp.zeros_like(state)
    for ahead in range(groups - 1, 0, -1):
        @pl.when(group >= ahead)
        def _():
            map_copy(ahead).wait_recv()
            block = maps[ahead].astype(F32)
            state[...] = chain(state[...], block) + block[:HEAD]

    behind = chain(state[...], early) + early[:HEAD]
    entering = jnp.where(first_member, state[...], behind)
    readout = local_read[...] + mm(carried[...], block_diagonal(entering, width), "enter", NT)
    head_means = jnp.where(head_blocks(width), 1.0 / HEAD, 0.0).astype(BF16)
    centred = readout - mm_left(readout, head_means)
    scaled = centred * lax.rsqrt(mm_left(centred * centred, head_means) + HEAD_EPS)
    mix_out[...] = (scaled * gate).astype(BF16)
    mix_copies = spread(mix_out, mix_slots, mix_send, mix_recv)
    copies[9].wait()
    result = gather(result, mix_out, mix_slots, mix_copies, ao_buf, width)
    out[...] = result.astype(BF16)
    for copy in conv_copies + mix_copies:
        copy.wait_send()
    for ahead in range(1, groups):
        @pl.when(group + ahead < groups)
        def _():
            map_copy(ahead).wait_send()


def local(
    n_sp, n_tp,
    tokens, input_norm_gain, convolution_value_weight, convolution_gate_weight,
    depthwise_taps_weight, convolution_group_gain, convolution_group_shift,
    receptance_weight, key_weight, value_weight, decay_weight, correction_rate_weight,
    output_gate_weight, key_prenorm_gain, decay_offset_bias, position_decay_shift,
    extra_log_decay, head_norm_gain, convolution_output_weight, attention_output_weight,
):
    rows, model = tokens.shape
    channels = convolution_value_weight.shape[1]
    width = key_weight.shape[1]
    vmem = pl.BlockSpec(memory_space=pltpu.VMEM)
    anywhere = pl.BlockSpec(memory_space=pl.ANY)

    def line(values):
        return values.reshape(1, -1)

    weights = (
        convolution_value_weight, convolution_gate_weight, key_weight, receptance_weight,
        decay_weight, correction_rate_weight, value_weight, output_gate_weight,
        convolution_output_weight, attention_output_weight,
    )
    span = rows // n_tp
    halo_rows = -(-(depthwise_taps_weight.shape[0] - 1) // 16) * 16
    groups = n_sp // 2
    dma = pltpu.SemaphoreType.DMA
    map_shape = (2 * HEAD, width)
    return pl.pallas_call(
        functools.partial(layer_kernel, n_sp, n_tp),
        name="layer",
        out_shape=jax.ShapeDtypeStruct((span, model), BF16),
        in_specs=[vmem] * 10 + [anywhere] * 10,
        out_specs=vmem,
        scratch_shapes=[pltpu.VMEM(weight.shape, BF16) for weight in weights]
        + [
            pltpu.VMEM((rows, channels), BF16),
            pltpu.VMEM((halo_rows + rows, channels), F32),
            pltpu.VMEM((halo_rows, channels), BF16),
            pltpu.VMEM(map_shape, WIRE),
            pltpu.VMEM(map_shape, WIRE),
            pltpu.VMEM(map_shape, WIRE),
            pltpu.VMEM((groups,) + map_shape, WIRE),
            pltpu.VMEM((HEAD, width), F32),
            pltpu.VMEM((rows, width), F32),
            pltpu.VMEM((rows, width), F32),
            pltpu.VMEM((rows, channels), BF16),
            pltpu.VMEM((rows, width), BF16),
            pltpu.VMEM((n_tp, span, channels), BF16),
            pltpu.VMEM((n_tp, span, width), BF16),
            dma((10,)), dma((2,)), dma((2,)), dma((groups,)), dma((groups,)),
            dma((n_tp,)), dma((n_tp,)), dma((n_tp,)), dma((n_tp,)),
        ],
        compiler_params=pltpu.CompilerParams(
            collective_id=0, has_side_effects=True, vmem_limit_bytes=VMEM_LIMIT
        ),
    )(
        tokens, line(input_norm_gain), line(key_prenorm_gain), line(decay_offset_bias),
        position_decay_shift, extra_log_decay, depthwise_taps_weight,
        line(convolution_group_gain), line(convolution_group_shift), line(head_norm_gain),
        *weights,
    )


def solution(mesh):
    in_specs = (
        P("sp", None),
        P(),
        P(None, "tp"),
        P(None, "tp"),
        P(None, "tp"),
        P("tp"),
        P("tp"),
        P(None, "tp"),
        P(None, "tp"),
        P(None, "tp"),
        P(None, "tp"),
        P(None, "tp"),
        P(None, "tp"),
        P("tp"),
        P("tp"),
        P("sp", "tp"),
        P("sp", "tp"),
        P("tp"),
        P(),
        P(),
    )
    body = functools.partial(local, mesh.shape["sp"], mesh.shape["tp"])
    return jax.shard_map(
        body, mesh=mesh, in_specs=in_specs, out_specs=P(("sp", "tp"), None), check_vma=False
    )
```

time: 38.2 us -> 32 us (0.84)
  the two profiles are of different devices: /device:TPU:25 before, /device:TPU:0 now
where the time goes in v2:
time: 32 us; the launch traced here: 31.8 us
  Pallas kernels  30.1 us (94%)
  local copies, waits for them, and re-layouts  1.67 us (5%)
    pallas_call x1, Pallas kernels, local(): pl.pallas_call(functools.partial(layer_kernel, n_sp, n_tp), name='layer',...  30.1 us
    unnamed x1, local copies, waits for them, and re-layouts  1.67 us

profile of v2, /device:TPU:0, one launch (start us, length us, event | category | flops | bytes accessed | tf_op | source)
XLA Modules:
  0.0 31.8 jit_solution(10457478760824305572)
XLA Ops:
  0.0 30.1 %layer.1 = bf16[64,2048]{1,0:T(8,128)(2,1)} custom-call(bf16[256,2048]{1,0:T(8,128)(2,1)} %tok.1, f32[1,2048]{1,0:T(1,128)} %bitcast.6, f32[1,256]{1,0:T(1,128)} %bitcast.7, f32[1,256]{1,0:T(1,128)} %bitcast.8, f32[256,256]{1,0:T(8,128)} %shift.1, f32[256,256]{1,0:T(8,128)} %extra.1, f32[31,128]{1,0:T(8,128)} %taps.1, f32[1,128]{1,0:T(1,128)} %bitcast.10, ...), custom_call_target="tpu_custom_call" | custom-call | tf_op jit(solution)/shard_map/layer/pallas_call | solution.py:418
  30.1 1.7 %copy.22 = bf16[64,2048]{1,0:T(8,128)(2,1)} copy(bf16[64,2048]{1,0:T(8,128)(2,1)} %layer.1) | data formatting | bytes 524288

commit v3 on v2

--- a/solution.py
+++ b/solution.py
@@ -88,26 +88,18 @@
 
 def layer_kernel(
     n_sp, n_tp,
-    tok, gain, kgain, bias, shift, extra, taps, ggain, gshift, hgain,
-    wcv, wcg, wk, wr, wd, we, wv, wg, wco, wao,
+    gain, kgain, bias, taps, ggain, gshift, hgain,
+    tok_hbm, shift_hbm, extra_hbm, wcv, wcg, wk, wr, wd, we, wv, wg, wco, wao,
     out,
-    cv_buf, cg_buf, k_buf, r_buf, d_buf, e_buf, v_buf, g_buf, co_buf, ao_buf,
+    tok, shift, extra, cv_buf, cg_buf, k_buf, r_buf, d_buf, e_buf, v_buf, g_buf, co_buf, ao_buf,
     conv_in, extended, halo, own_map, partner_map, pair_map, maps, state,
     local_read, carried, conv_out, mix_out, conv_slots, mix_slots,
     weight_sem, halo_sem, pair_sem, map_send, map_recv, conv_send, conv_recv, mix_send, mix_recv,
 ):
     sp, tp = lax.axis_index("sp"), lax.axis_index("tp")
-    barrier = pltpu.get_barrier_semaphore()
-    for step in range(1, n_sp):
-        pl.semaphore_signal(
-            barrier, inc=1, device_id=(lax.rem(sp + step, n_sp), tp), device_id_type=MESH
-        )
-    for step in range(1, n_tp):
-        pl.semaphore_signal(
-            barrier, inc=1, device_id=(sp, lax.rem(tp + step, n_tp)), device_id_type=MESH
-        )
     order = (
-        (wk, k_buf), (we, e_buf), (wd, d_buf), (wv, v_buf), (wcv, cv_buf), (wcg, cg_buf),
+        (tok_hbm, tok), (wk, k_buf), (we, e_buf), (shift_hbm, shift), (extra_hbm, extra),
+        (wd, d_buf), (wv, v_buf), (wcv, cv_buf), (wcg, cg_buf),
         (wr, r_buf), (wg, g_buf), (wco, co_buf), (wao, ao_buf),
     )
     copies = []
@@ -115,6 +107,15 @@
         copy = pltpu.make_async_copy(source, buffer, weight_sem.at[index])
         copy.start()
         copies.append(copy)
+    barrier = pltpu.get_barrier_semaphore()
+    for step in range(1, n_sp):
+        pl.semaphore_signal(
+            barrier, inc=1, device_id=(lax.rem(sp + step, n_sp), tp), device_id_type=MESH
+        )
+    for step in range(1, n_tp):
+        pl.semaphore_signal(
+            barrier, inc=1, device_id=(sp, lax.rem(tp + step, n_tp)), device_id_type=MESH
+        )
     rows = tok.shape[0]
     channels = conv_in.shape[1]
     width = local_read.shape[1]
@@ -124,6 +125,7 @@
     groups = n_sp // 2
     group, parity = sp // 2, lax.rem(sp, 2)
     first_member = parity == 0
+    copies[0].wait()
     x = tok[...].astype(F32)
     normed = (
         x * lax.rsqrt(jnp.mean(x * x, axis=-1, keepdims=True) + NORM_EPS) * gain[...]
@@ -133,12 +135,14 @@
         copies[index].wait()
         return dot(normed, order[index][1][...]).astype(BF16).astype(F32)
 
-    key_all = project(0)
+    key_all = project(1)
     ones = jnp.where(head_blocks(width), 1.0, 0.0).astype(BF16)
     unit = key_all * kgain[...]
     unit = unit * lax.rsqrt(mm_left(unit * unit, ones) + KEY_EPS)
-    erase = unit * jax.nn.sigmoid(project(1))
-    logits = project(2) + bias[...] + shift[...]
+    erase = unit * jax.nn.sigmoid(project(2))
+    copies[3].wait()
+    copies[4].wait()
+    logits = project(5) + bias[...] + shift[...]
     decay = jax.nn.sigmoid(logits) * (-0.6065306597126334) + extra[...]
     row, col = iota2(PAIR, PAIR)
     same = (row // CHUNK) == (col // CHUNK)
@@ -170,7 +174,7 @@
     keep = jnp.exp(final - cum)
     kept_erase = erase * keep
     kept_key = key_all * keep
-    value = project(3)
+    value = project(6)
 
     units = [(h, p) for h in range(heads) for p in range(pairs)]
 
@@ -242,22 +246,27 @@
     )
     pair_copy.start()
 
-    conv_value = project(4)
-    conv_rows = (conv_value * jax.nn.sigmoid(project(5))).astype(BF16)
+    conv_value = project(7)
+    conv_rows = (conv_value * jax.nn.sigmoid(project(8))).astype(BF16)
     conv_in[...] = conv_rows
     halo_copy = pltpu.make_async_remote_copy(
         src_ref=conv_in.at[pl.ds(rows - halo_rows, halo_rows)], dst_ref=halo,
         send_sem=halo_sem.at[0], recv_sem=halo_sem.at[1],
-        device_id=(lax.rem(sp + 1, n_sp), tp), device_id_type=MESH,
-    )
-    halo_copy.start()
+        device_id=(sp + 1, tp), device_id_type=MESH,
+    )
+    has_next = sp + 1 < n_sp
+
+    @pl.when(has_next)
+    def _():
+        halo_copy.start()
+
     extended[halo_rows:, :] = conv_rows.astype(F32)
 
     def chain(carry, block):
         trans = block_diagonal(block[HEAD:], width)
         return mm(carry, trans, "enter")
 
-    receptance = project(6)
+    receptance = project(9)
     left_read = receptance * jnp.exp(cum - mid)
     query_read = receptance * jnp.exp(cum)
 
@@ -281,9 +290,15 @@
         def _():
             map_copy(ahead).start()
 
-    halo_copy.wait()
-    received = halo[...].astype(F32)
-    extended[:halo_rows, :] = jnp.where(sp == 0, 0.0, received)
+    @pl.when(sp > 0)
+    def _():
+        halo_copy.wait_recv()
+        extended[:halo_rows, :] = halo[...].astype(F32)
+
+    @pl.when(sp == 0)
+    def _():
+        extended[:halo_rows, :] = jnp.zeros((halo_rows, channels), F32)
+
     tap_count = taps.shape[0]
     total = jnp.zeros((rows, channels), F32)
     for offset in range(tap_count):
@@ -340,7 +355,7 @@
                 ) + mm(read[:, HEAD:], prior, "carry", NT)
             local_read[start:start + CHUNK, lanes] = read[:, :HEAD]
             carried[start:start + CHUNK, lanes] = read[:, HEAD:]
-    gate = jax.nn.sigmoid(project(7)) * hgain[...]
+    gate = jax.nn.sigmoid(project(10)) * hgain[...]
 
     own = pl.multiple_of(tp * span, span)
 
@@ -356,7 +371,7 @@
             )
         return result
 
-    copies[8].wait()
+    copies[11].wait()
     result = gather(
         jnp.zeros(out.shape, F32), conv_out, conv_slots, conv_copies, co_buf, channels
     )
@@ -377,11 +392,16 @@
     scaled = centred * lax.rsqrt(mm_left(centred * centred, head_means) + HEAD_EPS)
     mix_out[...] = (scaled * gate).astype(BF16)
     mix_copies = spread(mix_out, mix_slots, mix_send, mix_recv)
-    copies[9].wait()
+    copies[12].wait()
     result = gather(result, mix_out, mix_slots, mix_copies, ao_buf, width)
     out[...] = result.astype(BF16)
     for copy in conv_copies + mix_copies:
         copy.wait_send()
+
+    @pl.when(has_next)
+    def _():
+        halo_copy.wait_send()
+
     for ahead in range(1, groups):
         @pl.when(group + ahead < groups)
         def _():
@@ -419,9 +439,14 @@
         functools.partial(layer_kernel, n_sp, n_tp),
         name="layer",
         out_shape=jax.ShapeDtypeStruct((span, model), BF16),
-        in_specs=[vmem] * 10 + [anywhere] * 10,
+        in_specs=[vmem] * 7 + [anywhere] * 13,
         out_specs=vmem,
-        scratch_shapes=[pltpu.VMEM(weight.shape, BF16) for weight in weights]
+        scratch_shapes=[
+            pltpu.VMEM(tokens.shape, BF16),
+            pltpu.VMEM(position_decay_shift.shape, F32),
+            pltpu.VMEM(extra_log_decay.shape, F32),
+        ]
+        + [pltpu.VMEM(weight.shape, BF16) for weight in weights]
         + [
             pltpu.VMEM((rows, channels), BF16),
             pltpu.VMEM((halo_rows + rows, channels), F32),
@@ -437,17 +462,16 @@
             pltpu.VMEM((rows, width), BF16),
             pltpu.VMEM((n_tp, span, channels), BF16),
             pltpu.VMEM((n_tp, span, width), BF16),
-            dma((10,)), dma((2,)), dma((2,)), dma((groups,)), dma((groups,)),
+            dma((13,)), dma((2,)), dma((2,)), dma((groups,)), dma((groups,)),
             dma((n_tp,)), dma((n_tp,)), dma((n_tp,)), dma((n_tp,)),
         ],
         compiler_params=pltpu.CompilerParams(
             collective_id=0, has_side_effects=True, vmem_limit_bytes=VMEM_LIMIT
         ),
     )(
-        tokens, line(input_norm_gain), line(key_prenorm_gain), line(decay_offset_bias),
-        position_decay_shift, extra_log_decay, depthwise_taps_weight,
-        line(convolution_group_gain), line(convolution_group_shift), line(head_norm_gain),
-        *weights,
+        line(input_norm_gain), line(key_prenorm_gain), line(decay_offset_bias),
+        depthwise_taps_weight, line(convolution_group_gain), line(convolution_group_shift),
+        line(head_norm_gain), tokens, position_decay_shift, extra_log_decay, *weights,
     )
 
 

time: 32 us -> 28.6 us (0.89)
  Pallas kernels: 30.1 us -> 26.8 us
    pallas_call x1, Pallas kernels: 30.1 us -> 26.8 us  [local(): pl.pallas_call(functools.partial(layer_kernel, n_sp, n_tp), name='layer',...]
where the time goes in v3:
time: 28.6 us; the launch traced here: 28.4 us
  Pallas kernels  26.8 us (94%)
  local copies, waits for them, and re-layouts  1.67 us (6%)
    pallas_call x1, Pallas kernels, local(): pl.pallas_call(functools.partial(layer_kernel, n_sp, n_tp), name='layer',...  26.8 us
    unnamed x1, local copies, waits for them, and re-layouts  1.67 us

profile of v3, /device:TPU:0, one launch (start us, length us, event | category | flops | bytes accessed | tf_op | source)
XLA Modules:
  0.0 28.4 jit_solution(10822473628144250412)
XLA Ops:
  0.0 26.8 %layer.1 = bf16[64,2048]{1,0:T(8,128)(2,1)} custom-call(f32[1,2048]{1,0:T(1,128)} %bitcast.6, f32[1,256]{1,0:T(1,128)} %bitcast.7, f32[1,256]{1,0:T(1,128)} %bitcast.8, f32[31,128]{1,0:T(8,128)} %taps.1, f32[1,128]{1,0:T(1,128)} %bitcast.10, f32[1,128]{1,0:T(1,128)} %bitcast.11, f32[1,256]{1,0:T(1,128)} %bitcast.9, bf16[256,2048]{1,0:T(8,128)(2,1)} %tok_hbm.1, ...), custom_call_target="tpu_custom_call" | custom-call | tf_op jit(solution)/shard_map/layer/pallas_call | solution.py:438
  26.8 1.7 %copy.22 = bf16[64,2048]{1,0:T(8,128)(2,1)} copy(bf16[64,2048]{1,0:T(8,128)(2,1)} %layer.1) | data formatting | bytes 524288
